TPU v7x, 128 devices: a whole 4x4x4 slice. The times are simulated.
128 devices in a mesh: sp: 16 (over z, y), tp: 8 (over x, core).
Axes of the slice: x: 4, y: 4, z: 4, core: 2. Of those that a mesh axis runs over, the one named last changes fastest.
Arguments:
- query_proj: bfloat16 [16384, 2048], P('sp', 'tp'), may hold values from -6 to 6
- key_proj: bfloat16 [16384, 2048], P('sp', 'tp'), may hold values from -6 to 6
- value_proj: bfloat16 [16384, 4096], P('sp', 'tp'), may hold values from -6 to 6
- gate_proj: bfloat16 [16384, 4096], P('sp', 'tp'), may hold values from -6 to 6
- log_decay: float32 [16384, 8], P('sp', 'tp'), may hold values from -0.75 to 0, as said below
- residual: bfloat16 [16384, 2048], P('sp'), may hold values from -4 to 4
- out_weight: bfloat16 [4096, 2048], P('tp'), may hold values from -0.09375 to 0.09375
- norm_gain: float32 [2, 2048], replicated, may hold values from 0.1 to 1.9
- norm_bias: float32 [2, 2048], replicated, may hold values from -1.5 to 1.5
- up_gate: bfloat16 [2048, 5632], P('sp', 'tp'), may hold values from -0.125 to 0.125
- up_value: bfloat16 [2048, 5632], P('sp', 'tp'), may hold values from -0.125 to 0.125
- conv_weight: float32 [2, 3, 5632], P(None, None, 'tp'), may hold values from -3 to 3
- conv_bias: float32 [2, 5632], P(None, 'tp'), may hold values from -1.5 to 1.5
- down_weight: bfloat16 [5632, 2048], P('tp', 'sp'), may hold values from -0.078125 to 0.078125
Outputs:
- layer_output: bfloat16 [16384, 2048], P(('sp', 'tp'))
Inputs may be any that keep to these rules, and one draw needn't show every extreme that they name: `log_decay`: all entries are negative.
All inputs are finite; a program needn't handle non-finite values.
Results may differ from a plain program's by a relative error of at most 0.023.
Values may be sent and summed in bfloat16 or wider, within the bound.
No kernel may reach another device: no remote copies, remote signals or barrier semaphores. Data moves between devices by JAX's collectives and lax.ppermute only.
A program may use at most 128 MiB of HBM per device.

v0:
```python
import jax
import jax.numpy as jnp
from jax import lax
from jax.sharding import Mesh
from jax.sharding import PartitionSpec as P

BLOCK = 256
SP = ("sp_0", "sp_1")
SP_TP = ("sp_0", "sp_1", "tp")
alpha_scale = 8.0**0.25
rope_base = 10000.0
tiny_stabilizer = 1e-05


def turned_gather(arrays, axis, dims):
    turned = [jnp.moveaxis(a, dim, 0) for a, dim in zip(arrays, dims)]
    both = jnp.concatenate([t.reshape(len(t), -1) for t in turned], axis=1)
    out, at, finished = (lax.all_gather(both, axis, axis=0, tiled=True), 0, [])
    for t, dim in zip(turned, dims):
        piece = out[:, at : at + t[0].size].reshape(-1, *t.shape[1:])
        finished.append(jnp.moveaxis(piece, 0, dim))
        at += t[0].size
    return tuple(finished)


def neutral_like(x, identity):
    return jax.tree.map(
        lambda a, e: jnp.broadcast_to(jnp.asarray(e, a.dtype), a.shape), x, identity
    )


def entering(x, axes, combine, identity):
    before = start = neutral_like(x, identity)
    subtotal = x
    for axis in reversed(axes):
        length, position = (lax.axis_size(axis), lax.axis_index(axis))
        pieces = jax.tree.map(
            lambda part, kind: lax.all_gather(part.astype(kind), axis),
            subtotal,
            (jnp.bfloat16, jnp.bfloat16),
        )
        inside, subtotal = (start, start)
        for k in range(length):
            passed = k < position
            subtotal = combine(
                subtotal, jax.tree.map(lambda part, own: part[k].astype(own.dtype), pieces, x)
            )
            inside = jax.tree.map(lambda new, old: jnp.where(passed, new, old), subtotal, inside)
        before = combine(inside, before)
    return before


def passed_along(x, axis, by):
    length = lax.axis_size(axis)
    pairs = [(i, i + by) for i in range(length) if 0 <= i + by < length]
    return lax.ppermute(x, axis, pairs)


def rotate(vectors, positions):
    head_width = vectors.shape[-1]
    half_width = head_width // 2
    inverse_freq = rope_base ** (-2.0 * jnp.arange(half_width, dtype=jnp.float32) / head_width)
    angles = positions[:, None] * inverse_freq[None, :]
    cosine = jnp.cos(angles)[:, None, :]
    sine_part = jnp.sin(angles)[:, None, :]
    front = vectors[..., :half_width]
    second = vectors[..., half_width:]
    return jnp.concatenate(
        [front * cosine - second * sine_part, front * sine_part + second * cosine], axis=-1
    )


def layer_norm(values, gain, shift):
    average = values.mean(-1, keepdims=True)
    spread = jnp.square(values - average).mean(-1, keepdims=True)
    return (values - average) * lax.rsqrt(spread + tiny_stabilizer) * gain + shift


def block_parts(query_tile, lookup_piece, payload_piece, log_blk):
    cum_log = jnp.cumsum(log_blk, axis=0)
    cum_heads = cum_log.T
    log_gap = cum_heads[:, :, None] - cum_heads[:, None, :]
    offsets = jnp.arange(log_blk.shape[0])
    causal = (offsets[:, None] >= offsets[None, :])[None]
    weight = jnp.where(causal, jnp.exp(jnp.where(causal, log_gap, 0.0)), 0.0)
    score_matrix = jnp.einsum(
        "jka,ska->kjs", query_tile, lookup_piece, preferred_element_type=jnp.float32
    )
    segment_scaling = (score_matrix * weight).astype(jnp.bfloat16)
    within = jnp.einsum(
        "htm,mhe->the", segment_scaling, payload_piece, preferred_element_type=jnp.float32
    )
    block_total = cum_log[-1]
    to_end = jnp.exp(block_total[None, :] - cum_log)
    faded_lookup_vector = (lookup_piece.astype(jnp.float32) * to_end[:, :, None]).astype(
        jnp.bfloat16
    )
    summand_term = jnp.einsum(
        "ajo,ajd->jod", faded_lookup_vector, payload_piece, preferred_element_type=jnp.float32
    )
    scaled_query = (query_tile.astype(jnp.float32) * jnp.exp(cum_log)[:, :, None]).astype(
        jnp.bfloat16
    )
    return (within, scaled_query, summand_term, jnp.exp(block_total))


def causal_conv(rows, edge_rows, taps, shift):
    padded = jnp.concatenate([edge_rows, rows], axis=0).astype(jnp.float32)
    length = rows.shape[0]
    result = shift[None, :] + padded[0:length] * taps[0]
    result = result + padded[1 : length + 1] * taps[1]
    return result + padded[2 : length + 2] * taps[2]


def combine(earlier, later):
    return (earlier[0] * later[0], later[0][:, None, None] * earlier[1] + later[1])


def shards(
    query_proj,
    key_proj,
    value_proj,
    gate_proj,
    log_decay,
    residual,
    out_weight,
    norm_gain,
    norm_bias,
    up_gate,
    up_value,
    conv_weight,
    conv_bias,
    down_weight,
):
    tok_rows = query_proj.shape[0]
    head_count = log_decay.shape[1]
    key_width = query_proj.shape[1] // head_count
    value_width = value_proj.shape[1] // head_count
    full_gate, full_value, full_down = turned_gather(
        (up_gate, up_value, down_weight), SP, (0, 0, 1)
    )
    positions = (lax.axis_index(SP) * tok_rows + jnp.arange(tok_rows)).astype(jnp.float32)
    query_rot = rotate(
        query_proj.astype(jnp.float32).reshape(tok_rows, head_count, key_width), positions
    ).astype(jnp.bfloat16)
    key_rot = (
        rotate(key_proj.astype(jnp.float32).reshape(tok_rows, head_count, key_width), positions)
        * key_width ** (-0.5)
    ).astype(jnp.bfloat16)
    block_count = tok_rows // BLOCK
    asking_segments = query_rot.reshape(block_count, BLOCK, head_count, key_width)
    key_blocks = key_rot.reshape(block_count, BLOCK, head_count, key_width)
    value_blocks = value_proj.reshape(block_count, BLOCK, head_count, value_width)
    log_blocks = log_decay.reshape(block_count, BLOCK, head_count)
    within, scaled_query, summand_term, block_decay = jax.vmap(block_parts)(
        asking_segments, key_blocks, value_blocks, log_blocks
    )

    def absorb(carry_state, pieces):
        return (pieces[1][:, None, None] * carry_state + pieces[0], None)

    zero_state = jnp.zeros((head_count, key_width, value_width), jnp.float32)
    own_state, _ = lax.scan(absorb, zero_state, (summand_term, block_decay))
    own_decay = jnp.prod(block_decay, axis=0)
    _, incoming = entering(
        (own_decay, own_state), SP, combine, (jnp.ones_like(own_decay), zero_state)
    )

    def advance(carry_state, pieces):
        carried = jnp.einsum(
            "thd,hde->the",
            pieces[0],
            carry_state.astype(jnp.bfloat16),
            preferred_element_type=jnp.float32,
        )
        return (pieces[2][:, None, None] * carry_state + pieces[1], carried)

    _, carried = lax.scan(advance, incoming, (scaled_query, summand_term, block_decay))
    mixed_heads = (within + carried).reshape(tok_rows, head_count, value_width)
    average = mixed_heads.mean(-1, keepdims=True)
    spread = jnp.square(mixed_heads - average).mean(-1, keepdims=True)
    standardized_rows = (mixed_heads - average) * lax.rsqrt(spread + tiny_stabilizer)
    gate_heads = gate_proj.astype(jnp.float32).reshape(tok_rows, head_count, value_width)
    gated_rows = (
        (jax.nn.silu(gate_heads) * standardized_rows)
        .astype(jnp.bfloat16)
        .reshape(tok_rows, head_count * value_width)
    )
    own_count = tok_rows // lax.axis_size("tp")
    partial_rows = jnp.dot(gated_rows, out_weight, preferred_element_type=jnp.float32)
    attended = lax.psum_scatter(
        partial_rows.astype(jnp.bfloat16), "tp", scatter_dimension=0, tiled=True
    ).astype(jnp.float32)
    own_residual = lax.dynamic_slice_in_dim(
        residual, lax.axis_index("tp") * own_count, own_count, 0
    )
    normed_own = layer_norm(
        alpha_scale * own_residual.astype(jnp.float32) + attended, norm_gain[0], norm_bias[0]
    ).astype(jnp.bfloat16)
    whole_rows = lax.all_gather(normed_own, "tp", axis=0, tiled=True)
    gate_up = jnp.dot(whole_rows, full_gate, preferred_element_type=jnp.float32)
    value_up = jnp.dot(whole_rows, full_value, preferred_element_type=jnp.float32)
    gate_up = gate_up.astype(jnp.bfloat16)
    value_up = value_up.astype(jnp.bfloat16)
    edges = jnp.concatenate([gate_up[tok_rows - 2 :], value_up[tok_rows - 2 :]], axis=0)
    edges = passed_along(edges, SP, 1)
    gate_edge, value_edge = (edges[:2], edges[2:])
    gate_conv = causal_conv(gate_up, gate_edge, conv_weight[0], conv_bias[0])
    value_conv = causal_conv(value_up, value_edge, conv_weight[1], conv_bias[1])
    activated = (jax.nn.gelu(gate_conv) * value_conv).astype(jnp.bfloat16)
    partial_ffn = jnp.dot(activated, full_down, preferred_element_type=jnp.float32)
    ffn_out = lax.psum_scatter(
        partial_ffn.astype(jnp.bfloat16), "tp", scatter_dimension=0, tiled=True
    ).astype(jnp.float32)
    return layer_norm(
        alpha_scale * normed_own.astype(jnp.float32) + ffn_out, norm_gain[1], norm_bias[1]
    ).astype(jnp.bfloat16)


def solution(mesh):
    torus = Mesh(mesh.devices.reshape(4, 4, mesh.shape["tp"]), ("sp_0", "sp_1", "tp"))
    return jax.shard_map(
        shards,
        mesh=torus,
        in_specs=(
            P(SP, "tp"),
            P(SP, "tp"),
            P(SP, "tp"),
            P(SP, "tp"),
            P(SP, "tp"),
            P(SP, None),
            P("tp", None),
            P(),
            P(),
            P(SP, "tp"),
            P(SP, "tp"),
            P(None, None, "tp"),
            P(None, "tp"),
            P("tp", SP),
        ),
        out_specs=P(SP_TP, None),
        check_vma=False,
    )
```

profile of v0, /device:TPU:0, one launch (start us, length us, event | category | flops | bytes accessed | tf_op | source)
XLA Modules:
  0.0 314.5 jit_solution(11302256274251141249)
XLA Ops:
  7.4 2.4 reduce-window.6
  10.4 1.4 bitcast_convert_fusion
  11.8 3.1 fusion.56
  15.7 2.0 convolution_bitcast_fusion.1
  17.7 9.8 %while.24 = (s32[]{:T(128)}, f32[1,256,512]{2,1,0:T(8,128)S(1)}, f32[4,1]{0,1:T(1,128)S(1)}, f32[4,1,256,512]{3,2,1,0:T(8,128)}, s32[]{:T(128)}, /*index=5*/s32[]{:T(128)}) while((s32[]{:T(128)}, f32[1,256,512]{2,1,0:T(8,128)S(1)}, f32[4,1]{0,1:T(1,128)S(1)}, f32[4,1,256,512]{3,2,1,0:T(8,128)}, s32[]{:T(128)}, ...), condition=%wide.region_4.5_spmd.clone, body=%wide.region_3.4_spmd.clone.sunk | while | flops 393219 | bytes 1572971 | solution.py:163
  18.3 1.8 bitcast_add_fusion.8
  20.8 1.8 bitcast_add_fusion.8
  23.2 1.8 bitcast_add_fusion.8
  25.7 1.8 bitcast_add_fusion.8
  29.7 1.4 dynamic-update-slice
  31.0 10.8 %all-reduce = bf16[4]{0:T(256)(128)(2,1)S(1)} all-reduce(bf16[4]{0:T(256)(128)(2,1)S(1)} %dynamic-update-slice), channel_id=1, replica_groups=mesh['sp_0'=4,'sp_1'=4,'tp'=8] {'sp_1'}, use_global_device_ids=true, to_apply=%add | all-reduce | flops 4 | bytes 16
  43.2 11.9 %all-gather.13.cloned.1.call-done = bf16[4,256,512]{2,1,0:T(8,128)(2,1)} async-done(((bf16[1,256,512]{2,1,0:T(8,128)(2,1)}), bf16[4,256,512]{2,1,0:T(8,128)(2,1)}) %all-gather.13.cloned.1.call-update) | async-done | bytes 1048592 | tf_op jit(solution)/shard_map/all_gather | solution.py:38
  55.0 4.0 %fusion.70 = bf16[1,1,256,512]{3,2,1,0:T(8,128)(2,1)} fusion(f32[]{:T(128)} %bitcast.39, f32[]{:T(128)} %bitcast.40, f32[]{:T(128)} %bitcast.41, f32[]{:T(128)} %bitcast.42, bf16[4,256,512]{2,1,0:T(8,128)(2,1)} %all-gather.13.cloned.1.call-done), kind=kLoop, calls=%fused_computation.102 | loop fusion | flops 1572864 | bytes 1310736 | tf_op jit(solution)/shard_map/convert_element_type | solution.py:38
  60.4 1.4 dynamic-update-slice.1
  61.8 10.7 %all-reduce.1 = bf16[4]{0:T(256)(128)(2,1)S(1)} all-reduce(bf16[4]{0:T(256)(128)(2,1)S(1)} %dynamic-update-slice.1), channel_id=2, replica_groups=mesh['sp_0'=4,'sp_1'=4,'tp'=8] {'sp_0'}, use_global_device_ids=true, to_apply=%add.1 | all-reduce | flops 4 | bytes 16
  78.2 1.9 fusion.61
  80.2 3.6 %all-gather.7.cloned.1.call-done = bf16[4,1,256,512]{3,2,1,0:T(8,128)(2,1)} async-done(((bf16[1,1,256,512]{3,2,1,0:T(8,128)(2,1)}), bf16[4,1,256,512]{3,2,1,0:T(8,128)(2,1)}) %all-gather.7.cloned.1.call-update) | async-done | bytes 1048592 | tf_op jit(solution)/shard_map/all_gather | solution.py:38
  83.8 3.9 %fusion.69 = f32[1,256,512]{2,1,0:T(8,128)S(1)} fusion(bf16[4,1,256,512]{3,2,1,0:T(8,128)(2,1)} %all-gather.7.cloned.1.call-done, f32[]{:T(128)} %bitcast.39, f32[]{:T(128)} %bitcast.40, f32[]{:T(128)} %bitcast.41, f32[]{:T(128)} %bitcast.42, f32[]{:T(128)} %bitcast.33, f32[]{:T(128)S(6)} %convert.26, f32[]{:T(128)S(6)} %convert.27, f32[]{:T(128)} %bitcast.38, ...), kind=kLoop, calls=%fused_computation.99 | loop fusion | flops 4194304 | bytes 2621484 | tf_op jit(solution)/shard_map/add | solution.py:116
  87.7 17.8 %while.23 = (s32[]{:T(128)}, f32[1,256,512]{2,1,0:T(8,128)S(1)}, f32[4,256,1,512]{3,1,2,0:T(8,128)}, f32[4,1]{0,1:T(1,128)S(1)}, f32[4,1,256,512]{3,2,1,0:T(8,128)}, /*index=5*/bf16[4,256,1,256]{3,1,2,0:T(8,128)(2,1)}, s32[]{:T(128)}) while((s32[]{:T(128)}, f32[1,256,512]{2,1,0:T(8,128)S(1)}, f32[4,256,1,512]{3,1,2,0:T(8,128)}, ...), condition=%wide.region_6.7_spmd, body=%wide.region_5.6_spmd.sunk | while | flops 67502080 | bytes 2753641 | solution.py:178
  88.4 1.9 fusion.118
  90.3 1.9 bitcast_add_fusion.7
  92.8 1.9 fusion.118
  94.7 1.9 bitcast_add_fusion.7
  97.2 1.9 fusion.118
  99.2 1.9 bitcast_add_fusion.7
  101.7 1.9 fusion.118
  103.6 1.9 bitcast_add_fusion.7
  105.5 4.2 %fusion.102 = (f32[4,256]{1,0:T(4,128)S(1)}, f32[4,256,1,512]{3,1,0,2:T(8,128)}) fusion(f32[4,256,1,512]{3,1,2,0:T(8,128)} %get-tuple-element.60, bf16[4,256,512]{2,1,0:T(8,128)(2,1)} %bitcast.150, bf16[4,256,128]{2,1,0:T(8,128)(2,1)} %bitcast.155, bf16[4,256,128]{2,1,0:T(8,128)(2,1)S(1)} %bitcast.153, f32[4,256]{1,0:T(4,128)S(1)} %get-tuple-element.145, ...), kind=kOutput, calls=%fused_computation.160 | convolution fusion | flops 406846464 | bytes 6889472 | tf_op jit(solution)/shard_map/vmap(htm,mhe->the)/dot_general | solution.py:90
  109.8 2.1 multiply_reduce_fusion
  112.0 2.2 fusion.31
  114.2 4.3 %convolution_convert_fusion.1 = bf16[1024,2048]{1,0:T(8,128)(2,1)} fusion(bf16[1024,512]{1,0:T(8,128)(2,1)S(1)} %fusion.31, bf16[512,2048]{1,0:T(8,128)(2,1)S(1)} %copy-done), kind=kOutput, calls=%fused_computation.14 | convolution fusion | flops 2149580800 | bytes 7340032 | tf_op jit(solution)/shard_map/dot_general | solution.py:190
  118.6 0.8 copy-done.5
  119.6 0.9 pad_maximum_fusion
  120.6 36.8 %reduce-scatter.3.cloned.1.call-done = bf16[128,2048]{1,0:T(8,128)(2,1)} async-done(((bf16[1024,2048]{1,0:T(8,128)(2,1)}), bf16[128,2048]{1,0:T(8,128)(2,1)}) %reduce-scatter.3.cloned.1.call-update) | async-done | bytes 524304 | tf_op jit(solution)/shard_map/reduce_scatter | solution.py:191
  157.4 1.5 fusion.45
  158.9 1.6 multiply_reduce_fusion.2
  160.4 2.4 add_convert_fusion.1
  163.1 36.6 %all-gather.11.cloned.1.call-done = bf16[2048,2112]{0,1:T(8,128)(2,1)} async-done(((bf16[128,2112]{0,1:T(8,128)(2,1)}), bf16[2048,2112]{0,1:T(8,128)(2,1)}) %all-gather.11.cloned.1.call-update) | async-done | bytes 8650768 | tf_op jit(solution)/shard_map/all_gather | solution.py:18
  199.7 32.7 %all-gather.9.cloned.1.call-done = bf16[1024,2048]{1,0:T(8,128)(2,1)} async-done(((bf16[128,2048]{1,0:T(8,128)(2,1)}), bf16[1024,2048]{1,0:T(8,128)(2,1)}) %all-gather.9.cloned.1.call-update) | async-done | bytes 4194320 | tf_op jit(solution)/shard_map/all_gather | solution.py:200
  232.4 6.4 %fusion.32 = bf16[1024,704]{0,1:T(8,128)(2,1)S(1)} fusion(bf16[1024,2048]{1,0:T(8,128)(2,1)} %all-gather.9.cloned.1.call-done, bf16[2048,2112]{0,1:T(8,128)(2,1)} %all-gather.11.cloned.1.call-done), kind=kOutput, calls=%fused_computation.52 | convolution fusion | flops 2953510912 | bytes 8519680 | tf_op jit(solution)/shard_map/dot_general | solution.py:201
  239.0 5.0 %fusion.35 = bf16[1024,704]{0,1:T(8,128)(2,1)S(1)} fusion(bf16[1024,2048]{1,0:T(8,128)(2,1)S(1)} %copy-done.12, bf16[2048,2112]{0,1:T(8,128)(2,1)} %all-gather.11.cloned.1.call-done), kind=kOutput, calls=%fused_computation.53 | convolution fusion | flops 2953510912 | bytes 8519680 | tf_op jit(solution)/shard_map/dot_general | solution.py:202
  244.3 3.6 %collective-permute-start = (bf16[4,704]{0,1:T(8,128)(2,1)S(1)}, bf16[4,704]{0,1:T(8,128)(2,1)S(1)}, u32[]{:S(2)}, u32[]{:S(2)}) collective-permute-start(bf16[4,704]{0,1:T(8,128)(2,1)S(1)} %pad_maximum_fusion.1), channel_id=1, source_target_pairs={{0,8},{8,16},{16,24},{24,32},{32,40},{40,48},{48,56},{56,64},{64,7... | collective-permute-start | bytes 16904 | tf_op jit(solution)/shard_map/ppermute | solution.py:56
  247.9 3.9 %collective-permute-done = bf16[4,704]{0,1:T(8,128)(2,1)S(1)} collective-permute-done((bf16[4,704]{0,1:T(8,128)(2,1)S(1)}, bf16[4,704]{0,1:T(8,128)(2,1)S(1)}, u32[]{:S(2)}, u32[]{:S(2)}) %collective-permute-start) | collective-permute-done | bytes 5664 | tf_op jit(solution)/shard_map/ppermute | solution.py:56
  253.5 10.0 %convolution_convert_fusion = bf16[1024,2048]{1,0:T(8,128)(2,1)} fusion(bf16[2048,2112]{0,1:T(8,128)(2,1)} %all-gather.11.cloned.1.call-done, f32[1026,704]{0,1:T(8,128)S(1)} %maximum_convert_fusion.1, f32[1026,704]{0,1:T(8,128)S(1)} %maximum_convert_fusion, f32[704]{0:T(1024)S(1)} %get-tuple-element.120, f32[704]{0:T(1024)S(1)} %get-tuple-element.121, ...), kind=kOutput, calls=%fused_computation.13 | convolution fusion | flops 2970746880 | bytes 24412160 | tf_op jit(solution)/shard_map/dot_general | solution.py:211
  263.6 38.9 %reduce-scatter.5.cloned.1.call-done = bf16[128,2048]{1,0:T(8,128)(2,1)} async-done(((bf16[1024,2048]{1,0:T(8,128)(2,1)}), bf16[128,2048]{1,0:T(8,128)(2,1)}) %reduce-scatter.5.cloned.1.call-update) | async-done | bytes 524304 | tf_op jit(solution)/shard_map/reduce_scatter | solution.py:212
  302.5 1.3 fusion.46
  303.8 1.4 multiply_reduce_fusion.1
  305.2 2.2 add_convert_fusion
  (91 shorter events, 13.9 us)
Async XLA Ops:
  7.4 106.8 %copy-start = (bf16[512,2048]{1,0:T(8,128)(2,1)S(1)}, bf16[512,2048]{1,0:T(8,128)(2,1)}, u32[]{:S(2)}) copy-start(bf16[512,2048]{1,0:T(8,128)(2,1)} %param.24) | copy-start | bytes 6291460
  7.4 47.7 %all-gather.13.cloned.1.call-start = ((), (), s32[]{:S(2)}) async-start(), calls=%async_computation.7 | async-start | bytes 1310720 | tf_op jit(solution)/shard_map/all_gather | solution.py:38
  10.4 5.3 %copy-start.4 = (bf16[1024,512]{1,0:T(8,128)(2,1)S(1)}, bf16[1024,512]{1,0:T(8,128)(2,1)}, u32[]{:S(2)}) copy-start(bf16[1024,512]{1,0:T(8,128)(2,1)} %param.20) | copy-start | bytes 3145732
  14.9 0.8 copy-start.3
  17.7 10.6 %copy-start.14 = (u32[128]{0:T(128)S(1)}, u32[128]{0:T(128)}, u32[]{:S(2)}) copy-start(u32[128]{0:T(128)} %constant.99) | copy-start | bytes 1540
  17.7 41.3 %copy-start.13 = (u32[128]{0:T(128)S(1)}, u32[128]{0:T(128)}, u32[]{:S(2)}) copy-start(u32[128]{0:T(128)} %constant.104) | copy-start | bytes 1540
  28.3 55.6 %all-gather.7.cloned.1.call-start = ((), (), s32[]{:S(2)}) async-start(), calls=%async_computation.2 | async-start | bytes 1310720 | tf_op jit(solution)/shard_map/all_gather | solution.py:38
  59.0 98.4 %reduce-scatter.3.cloned.1.call-start = ((), (), s32[]{:S(2)}) async-start(), calls=%async_computation.3 | async-start | bytes 4718592 | tf_op jit(solution)/shard_map/reduce_scatter | solution.py:191
  109.7 2.2 copy-start.1
  118.5 0.9 copy-start.5
  118.5 1.0 copy-start.6
  118.5 1.1 copy-start.7
  118.5 2.1 copy-start.9
  118.5 2.1 copy-start.10
  118.5 81.2 %all-gather.11.cloned.1.call-start = ((), (), s32[]{:S(2)}) async-start(), calls=%async_computation.5 | async-start | bytes 9191424 | tf_op jit(solution)/shard_map/all_gather | solution.py:18
  119.6 43.5 %copy-start.8 = (f32[2,3,704]{2,0,1:T(2,128)S(1)}, f32[2,3,704]{2,0,1:T(2,128)}, u32[]{:S(2)}) copy-start(f32[2,3,704]{2,0,1:T(2,128)} %param.29) | copy-start | bytes 50692
  120.5 111.9 %all-gather.9.cloned.1.call-start = ((), (), s32[]{:S(2)}) async-start(), calls=%async_computation.4 | async-start | bytes 4718592 | tf_op jit(solution)/shard_map/all_gather | solution.py:200
  162.8 139.7 %reduce-scatter.5.cloned.1.call-start = ((), (), s32[]{:S(2)}) async-start(), calls=%async_computation.6 | async-start | bytes 4718592 | tf_op jit(solution)/shard_map/reduce_scatter | solution.py:212
  232.4 6.5 %copy-start.12 = (bf16[1024,2048]{1,0:T(8,128)(2,1)S(1)}, bf16[1024,2048]{1,0:T(8,128)(2,1)}, u32[]{:S(2)}) copy-start(bf16[1024,2048]{1,0:T(8,128)(2,1)} %all-gather.9.cloned.1.call-done) | copy-start | bytes 12582916
  239.0 8.9 %copy-start.11 = (f32[2,704]{1,0:T(2,128)S(1)}, f32[2,704]{1,0:T(2,128)}, u32[]{:S(2)}) copy-start(f32[2,704]{1,0:T(2,128)} %param.30) | copy-start | bytes 16900
  244.3 7.6 %collective-permute-start = (bf16[4,704]{0,1:T(8,128)(2,1)S(1)}, bf16[4,704]{0,1:T(8,128)(2,1)S(1)}, u32[]{:S(2)}, u32[]{:S(2)}) collective-permute-start(bf16[4,704]{0,1:T(8,128)(2,1)S(1)} %pad_maximum_fusion.1), channel_id=1, source_target_pairs={{0,8},{8,16},{16,24},{24,32},{32,40},{40,48},{48,56},{56,64},{64,7... | collective-permute-start | bytes 16904 | tf_op jit(solution)/shard_map/ppermute | solution.py:56
  263.5 39.0 %copy-start.2 = (bf16[128,2048]{1,0:T(8,128)(2,1)S(1)}, bf16[128,2048]{1,0:T(8,128)(2,1)}, u32[]{:S(2)}) copy-start(bf16[128,2048]{1,0:T(8,128)(2,1)} %add_convert_fusion.1) | copy-start | bytes 1572868
Sparse Core Ops, SparseCore 0:
  28.4 26.5 all-gather.12
  59.1 24.6 all-gather.6
  118.7 38.6 reduce-scatter.2
  263.7 38.7 reduce-scatter.4
Sparse Core Ops, SparseCore 1:
  121.1 78.5 all-gather.10
  201.3 31.1 all-gather.8
where the time goes:
time: 316 us; the launch traced here: 314 us
  waiting for transfers between devices  165 us (52%)
  other arithmetic  51.6 us (16%)
  matrix products  39.7 us (13%)
  blocking collectives  21.5 us (7%)
  between operations  20.6 us (7%)
  local copies, waits for them, and re-layouts  12.4 us (4%)
  starting transfers between devices  4.01 us (1%)
    reduce_scatter x1, waiting for transfers between devices, shards(): lax.psum_scatter(partial_ffn.astype(jnp.bfloat16), 'tp', scatter_dimensio...  38.9 us
    reduce_scatter x1, waiting for transfers between devices, shards(): lax.psum_scatter(partial_rows.astype(jnp.bfloat16), 'tp', scatter_dimensi...  36.8 us
    all_gather x1, waiting for transfers between devices, turned_gather(): out, at, finished = (lax.all_gather(both, axis, axis=0, tiled=True), 0, [])  36.6 us
    all_gather x1, waiting for transfers between devices, shards(): whole_rows = lax.all_gather(normed_own, 'tp', axis=0, tiled=True)  32.7 us
    unnamed x2, blocking collectives  21.5 us
    all_gather x2, waiting for transfers between devices, entering(): lax.all_gather(part.astype(kind), axis)  15.5 us
    dot_general x1, matrix products, shards(): jnp.dot(activated, full_down, preferred_element_type=jnp.float32)  10 us
    dot_general x4, matrix products, advance(): jnp.einsum('thd,hde->the', pieces[0], carry_state.astype(jnp.bfloat16), p...  7.74 us
  transfers between devices with their start and end apart: 7, of which 7 were waited for; matrix products, arithmetic and copies ran while one was open for 5% of the time, Pallas kernels for 0%

commit v1 on v0

--- a/solution.py
+++ b/solution.py
@@ -10,6 +10,11 @@
 alpha_scale = 8.0**0.25
 rope_base = 10000.0
 tiny_stabilizer = 1e-05
+
+
+def all_by_exchange(shard, axis, along):
+    sent = jnp.stack([shard] * lax.axis_size(axis))
+    return jnp.concatenate(lax.all_to_all(sent, axis, 0, 0), axis=along)
 
 
 def turned_gather(arrays, axis, dims):
@@ -197,7 +202,7 @@
     normed_own = layer_norm(
         alpha_scale * own_residual.astype(jnp.float32) + attended, norm_gain[0], norm_bias[0]
     ).astype(jnp.bfloat16)
-    whole_rows = lax.all_gather(normed_own, "tp", axis=0, tiled=True)
+    whole_rows = all_by_exchange(normed_own, "tp", 0)
     gate_up = jnp.dot(whole_rows, full_gate, preferred_element_type=jnp.float32)
     value_up = jnp.dot(whole_rows, full_value, preferred_element_type=jnp.float32)
     gate_up = gate_up.astype(jnp.bfloat16)

time: 316 us -> 302 us (0.956)
  waiting for transfers between devices: 165 us -> 144 us
  starting transfers between devices: 4.01 us -> 8.19 us
    all_to_all x0 -> x1, waiting for transfers between devices: none -> 49.3 us  [all_by_exchange(): return jnp.concatenate(lax.all_to_all(sent, axis, 0, 0), axis=along)]
    all_gather x1, waiting for transfers between devices: 36.6 us -> 0.01 us  [turned_gather(): out, at, finished = (lax.all_gather(both, axis, axis=0, tiled=True), 0, [])]
    all_gather x1 -> x0, waiting for transfers between devices: 32.7 us -> none  [shards(): whole_rows = lax.all_gather(normed_own, 'tp', axis=0, tiled=True)]
    all_to_all x0 -> x1, starting transfers between devices: none -> 4.72 us  [all_by_exchange(): return jnp.concatenate(lax.all_to_all(sent, axis, 0, 0), axis=along)]
  transfers between devices with their start and end apart: 7 -> 7, of which waited for: 7 -> 6; matrix products, arithmetic and copies ran while one was open for 5% -> 6% of each run, Pallas kernels for 0% -> 0%
where the time goes in v1:
time: 302 us; the launch traced here: 301 us
  waiting for transfers between devices  144 us (48%)
  other arithmetic  50.8 us (17%)
  matrix products  40.8 us (14%)
  blocking collectives  21.5 us (7%)
  between operations  20.6 us (7%)
  local copies, waits for them, and re-layouts  14.9 us (5%)
  starting transfers between devices  8.19 us (3%)
    all_to_all x1, waiting for transfers between devices, all_by_exchange(): return jnp.concatenate(lax.all_to_all(sent, axis, 0, 0), axis=along)  49.3 us
    reduce_scatter x1, waiting for transfers between devices, shards(): lax.psum_scatter(partial_ffn.astype(jnp.bfloat16), 'tp', scatter_dimensio...  38.6 us
    reduce_scatter x1, waiting for transfers between devices, shards(): lax.psum_scatter(partial_rows.astype(jnp.bfloat16), 'tp', scatter_dimensi...  36.8 us
    unnamed x2, blocking collectives  21.5 us
    all_gather x2, waiting for transfers between devices, entering(): lax.all_gather(part.astype(kind), axis)  15.5 us
    dot_general x1, matrix products, shards(): jnp.dot(activated, full_down, preferred_element_type=jnp.float32)  9.99 us
    dot_general x4, matrix products, advance(): jnp.einsum('thd,hde->the', pieces[0], carry_state.astype(jnp.bfloat16), p...  7.74 us
    add x4, other arithmetic, advance(): return (pieces[2][:, None, None] * carry_state + pieces[1], carried)  7.52 us
  transfers between devices with their start and end apart: 7, of which 6 were waited for; matrix products, arithmetic and copies ran while one was open for 6% of the time, Pallas kernels for 0%

profile of v1, /device:TPU:0, one launch (start us, length us, event | category | flops | bytes accessed | tf_op | source)
XLA Modules:
  0.0 300.7 jit_solution(2947872717915264978)
XLA Ops:
  7.4 2.4 reduce-window.6
  10.4 1.4 bitcast_convert_fusion
  11.8 3.1 %fusion.56 = (bf16[1024,1,128]{2,0,1:T(8,128)(2,1)S(1)}, bf16[1024,1,128]{2,0,1:T(8,128)(2,1)}, f32[1024,1,128]{2,0,1:T(8,128)S(1)}, f32[1024,1,128]{2,0,1:T(8,128)S(1)}) fusion(f32[1024,1,256]{2,0,1:T(8,128)S(1)} %get-tuple-element.182, f32[128]{0:T(128)S(1)} %multiply_power_fusion, f32[1024]{0:T(1024)S(1)} %add_convert_fusion.2, ...), kind=kLoop, calls=%fused_computation.87 | loop fusion | flops 1966080 | bytes 3674624 | tf_op jit(solution)/shard_map/convert.17
  15.7 2.0 convolution_bitcast_fusion.1
  17.7 9.8 %while.24 = (s32[]{:T(128)}, f32[1,256,512]{2,1,0:T(8,128)S(1)}, f32[4,1]{0,1:T(1,128)S(1)}, f32[4,1,256,512]{3,2,1,0:T(8,128)}, s32[]{:T(128)}, /*index=5*/s32[]{:T(128)}) while((s32[]{:T(128)}, f32[1,256,512]{2,1,0:T(8,128)S(1)}, f32[4,1]{0,1:T(1,128)S(1)}, f32[4,1,256,512]{3,2,1,0:T(8,128)}, s32[]{:T(128)}, ...), condition=%wide.region_4.5_spmd.clone, body=%wide.region_3.4_spmd.clone.sunk | while | flops 393219 | bytes 1572971 | solution.py:168
  18.3 1.8 bitcast_add_fusion.8
  20.8 1.8 bitcast_add_fusion.8
  23.2 1.8 bitcast_add_fusion.8
  25.7 1.8 bitcast_add_fusion.8
  29.7 1.4 dynamic-update-slice
  31.0 10.8 %all-reduce = bf16[4]{0:T(256)(128)(2,1)S(1)} all-reduce(bf16[4]{0:T(256)(128)(2,1)S(1)} %dynamic-update-slice), channel_id=1, replica_groups=mesh['sp_0'=4,'sp_1'=4,'tp'=8] {'sp_1'}, use_global_device_ids=true, to_apply=%add | all-reduce | flops 4 | bytes 16
  43.2 11.9 %all-gather.10.cloned.1.call-done = bf16[4,256,512]{2,1,0:T(8,128)(2,1)} async-done(((bf16[1,256,512]{2,1,0:T(8,128)(2,1)}), bf16[4,256,512]{2,1,0:T(8,128)(2,1)}) %all-gather.10.cloned.1.call-update) | async-done | bytes 1048592 | tf_op jit(solution)/shard_map/all_gather | solution.py:43
  55.0 4.0 %fusion.70 = bf16[1,1,256,512]{3,2,1,0:T(8,128)(2,1)} fusion(f32[]{:T(128)} %bitcast.39, f32[]{:T(128)} %bitcast.40, f32[]{:T(128)} %bitcast.41, f32[]{:T(128)} %bitcast.42, bf16[4,256,512]{2,1,0:T(8,128)(2,1)} %all-gather.10.cloned.1.call-done), kind=kLoop, calls=%fused_computation.102 | loop fusion | flops 1572864 | bytes 1310736 | tf_op jit(solution)/shard_map/convert_element_type | solution.py:43
  60.4 1.4 dynamic-update-slice.1
  61.8 10.7 %all-reduce.1 = bf16[4]{0:T(256)(128)(2,1)S(1)} all-reduce(bf16[4]{0:T(256)(128)(2,1)S(1)} %dynamic-update-slice.1), channel_id=2, replica_groups=mesh['sp_0'=4,'sp_1'=4,'tp'=8] {'sp_0'}, use_global_device_ids=true, to_apply=%add.1 | all-reduce | flops 4 | bytes 16
  78.2 1.9 fusion.61
  80.2 3.6 %all-gather.6.cloned.1.call-done = bf16[4,1,256,512]{3,2,1,0:T(8,128)(2,1)} async-done(((bf16[1,1,256,512]{3,2,1,0:T(8,128)(2,1)}), bf16[4,1,256,512]{3,2,1,0:T(8,128)(2,1)}) %all-gather.6.cloned.1.call-update) | async-done | bytes 1048592 | tf_op jit(solution)/shard_map/all_gather | solution.py:43
  83.8 3.9 %fusion.69 = f32[1,256,512]{2,1,0:T(8,128)S(1)} fusion(bf16[4,1,256,512]{3,2,1,0:T(8,128)(2,1)} %all-gather.6.cloned.1.call-done, f32[]{:T(128)} %bitcast.39, f32[]{:T(128)} %bitcast.40, f32[]{:T(128)} %bitcast.41, f32[]{:T(128)} %bitcast.42, f32[]{:T(128)} %bitcast.33, f32[]{:T(128)S(6)} %convert.26, f32[]{:T(128)S(6)} %convert.27, f32[]{:T(128)} %bitcast.38, ...), kind=kLoop, calls=%fused_computation.99 | loop fusion | flops 4194304 | bytes 2621484 | tf_op jit(solution)/shard_map/add | solution.py:121
  87.7 17.8 %while.23 = (s32[]{:T(128)}, f32[1,256,512]{2,1,0:T(8,128)S(1)}, f32[4,256,1,512]{3,1,2,0:T(8,128)}, f32[4,1]{0,1:T(1,128)S(1)}, f32[4,1,256,512]{3,2,1,0:T(8,128)}, /*index=5*/bf16[4,256,1,256]{3,1,2,0:T(8,128)(2,1)}, s32[]{:T(128)}) while((s32[]{:T(128)}, f32[1,256,512]{2,1,0:T(8,128)S(1)}, f32[4,256,1,512]{3,1,2,0:T(8,128)}, ...), condition=%wide.region_6.7_spmd, body=%wide.region_5.6_spmd.sunk | while | flops 67502080 | bytes 2753641 | solution.py:183
  88.4 1.9 fusion.118
  90.3 1.9 bitcast_add_fusion.7
  92.8 1.9 fusion.118
  94.7 1.9 bitcast_add_fusion.7
  97.2 1.9 fusion.118
  99.2 1.9 bitcast_add_fusion.7
  101.7 1.9 fusion.118
  103.6 1.9 bitcast_add_fusion.7
  105.5 4.2 %fusion.102 = (f32[4,256]{1,0:T(4,128)S(1)}, f32[4,256,1,512]{3,1,0,2:T(8,128)}) fusion(f32[4,256,1,512]{3,1,2,0:T(8,128)} %get-tuple-element.60, bf16[4,256,512]{2,1,0:T(8,128)(2,1)} %bitcast.151, bf16[4,256,128]{2,1,0:T(8,128)(2,1)} %bitcast.156, bf16[4,256,128]{2,1,0:T(8,128)(2,1)S(1)} %bitcast.154, f32[4,256]{1,0:T(4,128)S(1)} %get-tuple-element.145, ...), kind=kOutput, calls=%fused_computation.160 | convolution fusion | flops 406846464 | bytes 6889472 | tf_op jit(solution)/shard_map/vmap(htm,mhe->the)/dot_general | solution.py:95
  109.8 2.1 multiply_reduce_fusion
  112.0 2.2 fusion.31
  114.2 4.3 %convolution_convert_fusion.1 = bf16[1024,2048]{1,0:T(8,128)(2,1)} fusion(bf16[1024,512]{1,0:T(8,128)(2,1)S(1)} %fusion.31, bf16[512,2048]{1,0:T(8,128)(2,1)S(1)} %copy-done), kind=kOutput, calls=%fused_computation.14 | convolution fusion | flops 2149580800 | bytes 7340032 | tf_op jit(solution)/shard_map/dot_general | solution.py:195
  119.6 0.8 pad_maximum_fusion
  120.5 36.8 %reduce-scatter.3.cloned.1.call-done = bf16[128,2048]{1,0:T(8,128)(2,1)} async-done(((bf16[1024,2048]{1,0:T(8,128)(2,1)}), bf16[128,2048]{1,0:T(8,128)(2,1)}) %reduce-scatter.3.cloned.1.call-update) | async-done | bytes 524304 | tf_op jit(solution)/shard_map/reduce_scatter | solution.py:196
  157.4 1.5 fusion.45
  158.9 1.6 multiply_reduce_fusion.2
  160.4 1.6 add_convert_fusion.1
  162.0 2.5 stack.2
  164.5 4.7 %all-to-all-start = ((bf16[8,128,2048]{2,1,0:T(8,128)(2,1)}), bf16[8,128,2048]{2,1,0:T(8,128)(2,1)}, u32[]{:S(2)}, u32[]{:S(2)}) async-start(bf16[8,128,2048]{2,1,0:T(8,128)(2,1)} %stack.2), calls=%async_computation.1 | async-start | bytes 8388608 | tf_op jit(solution)/shard_map/all_to_all | solution.py:17
  169.5 49.3 %all-to-all-done = bf16[8,128,2048]{2,1,0:T(8,128)(2,1)} async-done(((bf16[8,128,2048]{2,1,0:T(8,128)(2,1)}), bf16[8,128,2048]{2,1,0:T(8,128)(2,1)}, u32[]{:S(2)}, u32[]{:S(2)}) %all-to-all-start) | async-done | bytes 4194336 | tf_op jit(solution)/shard_map/all_to_all | solution.py:17
  218.9 6.3 %fusion.32 = bf16[1024,704]{0,1:T(8,128)(2,1)S(1)} fusion(bf16[1024,2048]{1,0:T(8,128)(2,1)} %bitcast.59, bf16[2048,2112]{0,1:T(8,128)(2,1)} %all-gather.8.cloned.1.call-done), kind=kOutput, calls=%fused_computation.52 | convolution fusion | flops 2953510912 | bytes 8519680 | tf_op jit(solution)/shard_map/dot_general | solution.py:206
  225.3 6.3 %fusion.35 = bf16[1024,704]{0,1:T(8,128)(2,1)S(1)} fusion(bf16[1024,2048]{1,0:T(8,128)(2,1)} %bitcast.59, bf16[2048,2112]{0,1:T(8,128)(2,1)} %all-gather.8.cloned.1.call-done), kind=kOutput, calls=%fused_computation.53 | convolution fusion | flops 2953510912 | bytes 8519680 | tf_op jit(solution)/shard_map/dot_general | solution.py:207
  231.8 3.1 %collective-permute-start = (bf16[4,704]{0,1:T(8,128)(2,1)S(1)}, bf16[4,704]{0,1:T(8,128)(2,1)S(1)}, u32[]{:S(2)}, u32[]{:S(2)}) collective-permute-start(bf16[4,704]{0,1:T(8,128)(2,1)S(1)} %pad_maximum_fusion.1), channel_id=1, source_target_pairs={{0,8},{8,16},{16,24},{24,32},{32,40},{40,48},{48,56},{56,64},{64,7... | collective-permute-start | bytes 16904 | tf_op jit(solution)/shard_map/ppermute | solution.py:61
  235.0 3.5 %collective-permute-done = bf16[4,704]{0,1:T(8,128)(2,1)S(1)} collective-permute-done((bf16[4,704]{0,1:T(8,128)(2,1)S(1)}, bf16[4,704]{0,1:T(8,128)(2,1)S(1)}, u32[]{:S(2)}, u32[]{:S(2)}) %collective-permute-start) | collective-permute-done | bytes 5664 | tf_op jit(solution)/shard_map/ppermute | solution.py:61
  240.1 10.0 %convolution_convert_fusion = bf16[1024,2048]{1,0:T(8,128)(2,1)} fusion(bf16[2048,2112]{0,1:T(8,128)(2,1)} %all-gather.8.cloned.1.call-done, f32[1026,704]{0,1:T(8,128)S(1)} %maximum_convert_fusion.1, f32[1026,704]{0,1:T(8,128)S(1)} %maximum_convert_fusion, f32[704]{0:T(1024)S(1)} %get-tuple-element.120, f32[704]{0:T(1024)S(1)} %get-tuple-element.121, ...), kind=kOutput, calls=%fused_computation.13 | convolution fusion | flops 2970746880 | bytes 24412160 | tf_op jit(solution)/shard_map/dot_general | solution.py:216
  250.1 38.6 %reduce-scatter.5.cloned.1.call-done = bf16[128,2048]{1,0:T(8,128)(2,1)} async-done(((bf16[1024,2048]{1,0:T(8,128)(2,1)}), bf16[128,2048]{1,0:T(8,128)(2,1)}) %reduce-scatter.5.cloned.1.call-update) | async-done | bytes 524304 | tf_op jit(solution)/shard_map/reduce_scatter | solution.py:217
  288.7 1.3 fusion.46
  290.0 1.4 multiply_reduce_fusion.1
  291.4 2.2 add_convert_fusion
  (87 shorter events, 14.6 us)
Async XLA Ops:
  7.4 106.8 %copy-start = (bf16[512,2048]{1,0:T(8,128)(2,1)S(1)}, bf16[512,2048]{1,0:T(8,128)(2,1)}, u32[]{:S(2)}) copy-start(bf16[512,2048]{1,0:T(8,128)(2,1)} %param.24) | copy-start | bytes 6291460
  7.4 47.7 %all-gather.10.cloned.1.call-start = ((), (), s32[]{:S(2)}) async-start(), calls=%async_computation.7 | async-start | bytes 1310720 | tf_op jit(solution)/shard_map/all_gather | solution.py:43
  10.4 5.3 %copy-start.3 = (bf16[1024,512]{1,0:T(8,128)(2,1)S(1)}, bf16[1024,512]{1,0:T(8,128)(2,1)}, u32[]{:S(2)}) copy-start(bf16[1024,512]{1,0:T(8,128)(2,1)} %param.20) | copy-start | bytes 3145732
  14.9 0.8 copy-start.2
  17.7 10.6 %copy-start.12 = (u32[128]{0:T(128)S(1)}, u32[128]{0:T(128)}, u32[]{:S(2)}) copy-start(u32[128]{0:T(128)} %constant.99) | copy-start | bytes 1540
  17.7 41.3 %copy-start.11 = (u32[128]{0:T(128)S(1)}, u32[128]{0:T(128)}, u32[]{:S(2)}) copy-start(u32[128]{0:T(128)} %constant.104) | copy-start | bytes 1540
  28.3 55.6 %all-gather.6.cloned.1.call-start = ((), (), s32[]{:S(2)}) async-start(), calls=%async_computation.3 | async-start | bytes 1310720 | tf_op jit(solution)/shard_map/all_gather | solution.py:43
  59.0 98.4 %reduce-scatter.3.cloned.1.call-start = ((), (), s32[]{:S(2)}) async-start(), calls=%async_computation.4 | async-start | bytes 4718592 | tf_op jit(solution)/shard_map/reduce_scatter | solution.py:196
  109.7 2.2 copy-start.1
  118.5 0.9 copy-start.4
  118.5 1.0 copy-start.5
  118.5 1.1 copy-start.6
  118.5 2.0 copy-start.8
  118.5 2.0 copy-start.9
  118.5 100.3 %all-gather.8.cloned.1.call-start = ((), (), s32[]{:S(2)}) async-start(), calls=%async_computation.5 | async-start | bytes 9191424 | tf_op jit(solution)/shard_map/all_gather | solution.py:23
  164.5 5.0 %copy-start.7 = (f32[2,3,704]{2,0,1:T(2,128)S(1)}, f32[2,3,704]{2,0,1:T(2,128)}, u32[]{:S(2)}) copy-start(f32[2,3,704]{2,0,1:T(2,128)} %param.29) | copy-start | bytes 50692
  164.5 54.4 %all-to-all-start = ((bf16[8,128,2048]{2,1,0:T(8,128)(2,1)}), bf16[8,128,2048]{2,1,0:T(8,128)(2,1)}, u32[]{:S(2)}, u32[]{:S(2)}) async-start(bf16[8,128,2048]{2,1,0:T(8,128)(2,1)} %stack.2), calls=%async_computation.1 | async-start | bytes 8388608 | tf_op jit(solution)/shard_map/all_to_all | solution.py:17
  169.2 119.5 %reduce-scatter.5.cloned.1.call-start = ((), (), s32[]{:S(2)}) async-start(), calls=%async_computation.6 | async-start | bytes 4718592 | tf_op jit(solution)/shard_map/reduce_scatter | solution.py:217
  225.3 9.7 %copy-start.10 = (f32[2,704]{1,0:T(2,128)S(1)}, f32[2,704]{1,0:T(2,128)}, u32[]{:S(2)}) copy-start(f32[2,704]{1,0:T(2,128)} %param.30) | copy-start | bytes 16900
  231.8 6.6 %collective-permute-start = (bf16[4,704]{0,1:T(8,128)(2,1)S(1)}, bf16[4,704]{0,1:T(8,128)(2,1)S(1)}, u32[]{:S(2)}, u32[]{:S(2)}) collective-permute-start(bf16[4,704]{0,1:T(8,128)(2,1)S(1)} %pad_maximum_fusion.1), channel_id=1, source_target_pairs={{0,8},{8,16},{16,24},{24,32},{32,40},{40,48},{48,56},{56,64},{64,7... | collective-permute-start | bytes 16904 | tf_op jit(solution)/shard_map/ppermute | solution.py:61
Sparse Core Ops, SparseCore 0:
  28.4 26.5 all-gather.9
  59.1 24.6 all-gather.5
  118.7 38.6 reduce-scatter.2
  250.2 38.4 reduce-scatter.4
Sparse Core Ops, SparseCore 1:
  121.1 78.5 all-gather.7
